TPU v7x, 32 devices: a whole 2x2x4 slice. The times are simulated.
32 devices in a mesh: grp: 2 (over y), sp: 4 (over z), tp: 4 (over x, core).
Axes of the slice: x: 2, y: 2, z: 4, core: 2. Of those that a mesh axis runs over, the one named last changes fastest.
Arguments:
- queries_small: bfloat16 [2048, 1024], P(('grp', 'sp'), 'tp'), parts along dimension 0, may hold values from -6 to 6
- keys_small: bfloat16 [2048, 512], P(('grp', 'sp'), 'tp'), parts along dimension 0, may hold values from -6 to 6
- values_small: bfloat16 [2048, 512], P(('grp', 'sp'), 'tp'), parts along dimension 0, may hold values from -6 to 6
- queries_large: bfloat16 [2048, 1024], P(('grp', 'sp'), 'tp'), parts along dimension 0, may hold values from -6 to 6
- keys_large: bfloat16 [2048, 512], P(('grp', 'sp'), 'tp'), parts along dimension 0, may hold values from -6 to 6
- values_large: bfloat16 [2048, 512], P(('grp', 'sp'), 'tp'), parts along dimension 0, may hold values from -6 to 6
- query_gain_small: float32 [128], P('grp'), parts along dimension 0, may hold values from 1.2 to 12
- key_gain_small: float32 [128], P('grp'), parts along dimension 0, may hold values from 1.2 to 12
- query_gain_large: float32 [256], P('grp'), parts along dimension 0, may hold values from 1.2 to 12
- key_gain_large: float32 [256], P('grp'), parts along dimension 0, may hold values from 1.2 to 12
- residual_in: bfloat16 [2048, 2048], P(('grp', 'sp', 'tp')), parts along dimension 0, may hold values from -1.5 to 1.5
- out_weight_small: bfloat16 [1024, 2048], P('tp'), may hold values from -0.125 to 0.125
- out_weight_large: bfloat16 [1024, 2048], P('tp'), may hold values from -0.125 to 0.125
- norm_gain: float32 [2048], replicated, may hold values from 0.1 to 1.9
- routes: int32 [2048, 2], P(('grp', 'sp', 'tp')), parts along dimension 0, may hold values from 0 to 7, all different within a row; in each aligned block of 64 rows (0 to 63, 64 to 127, ...) at most 32 rows name the same one
- route_scores: float32 [2048, 2], P(('grp', 'sp', 'tp')), parts along dimension 0, may hold values from 0.05 to 1
- expert_gate: bfloat16 [8, 2048, 1024], P('sp', None, 'tp'), may hold values from -0.125 to 0.125
- expert_up: bfloat16 [8, 2048, 1024], P('sp', None, 'tp'), may hold values from -0.125 to 0.125
- expert_down: bfloat16 [8, 1024, 2048], P('sp', 'tp'), may hold values from -0.1875 to 0.1875
Outputs:
- result: bfloat16 [2048, 2048], P(('grp', 'sp', 'tp')), parts along dimension 0
There are 2 independent parts, one for each index of `grp`. A program takes and returns all parts, laid end to end along the dimension named above; an argument that names none is the same for every part. Nothing has to cross between parts.
Inputs may be any that keep to these rules, and one draw needn't show every extreme that they name: `routes`: each token names 2 different experts; within the rows of one device (aligned blocks of 64 tokens) no expert is named more than 32 times, a bound that some block reaches.
All inputs are finite; a program needn't handle non-finite values.
Results may differ from a plain program's by a relative error of at most 0.02.
The roundings to bfloat16 on the way count: a program that leaves them out, or rounds other values in their place, can miss the bound.
Values may be sent and summed in bfloat16 or wider, within the bound.
A program may use at most 128 MiB of HBM per device.

v0:
```python
import jax
import jax.numpy as jnp
from jax import lax
from jax.sharding import PartitionSpec as P

HS_SMALL = 64
HS_LARGE = 128
GRID_W = 64


theta_base = 10000.0
norm_eps = 1e-06
block_target = 1280


def grid_tables(offset, length, head_size):
    places = offset + jnp.arange(length, dtype=jnp.int32)
    grid_rows = (places // GRID_W).astype(jnp.float32)
    grid_cols = (places % GRID_W).astype(jnp.float32)
    rates = jnp.power(
        theta_base, -2.0 * jnp.arange(head_size // 4, dtype=jnp.float32) / (head_size // 2)
    )
    row_angles = grid_rows[:, None, None] * rates
    col_angles = grid_cols[:, None, None] * rates
    return (jnp.cos(row_angles), jnp.sin(row_angles), jnp.cos(col_angles), jnp.sin(col_angles))


def half_turn(segment, cosine, sine_part):
    half_size = segment.shape[-1] // 2
    leading = segment[..., :half_size]
    trailing = segment[..., half_size:]
    return jnp.concatenate(
        [leading * cosine - trailing * sine_part, trailing * cosine + leading * sine_part], axis=-1
    )


def grid_turn(vectors, tables):
    row_cos, row_sin, col_cos, col_sin = tables
    half_size = vectors.shape[-1] // 2
    return jnp.concatenate(
        [
            half_turn(vectors[..., :half_size], row_cos, row_sin),
            half_turn(vectors[..., half_size:], col_cos, col_sin),
        ],
        axis=-1,
    )


def normed_turn(raw_rows, gain, tables):
    widened = raw_rows.astype(jnp.float32)
    scaled = (
        widened * lax.rsqrt(jnp.mean(widened * widened, axis=-1, keepdims=True) + norm_eps) * gain
    )
    return grid_turn(scaled, tables).astype(jnp.bfloat16)


def block_rows(row_count, shard_rows):
    shards = row_count // shard_rows
    chosen = 1
    for factor in range(1, max(1, block_target // shard_rows) + 1):
        if shards % factor == 0:
            chosen = factor
    return chosen * shard_rows


def attend_block(state, queries, key_rows, value_rows):
    largest, weight_sum, accumulated = state
    head_size = queries.shape[-1]
    kv_local = queries.shape[1]
    key_heads = key_rows.reshape(key_rows.shape[0], kv_local, head_size)
    value_heads = value_rows.reshape(value_rows.shape[0], kv_local, head_size)
    scores = jnp.einsum(
        "qgrd,kgd->qgrk", queries, key_heads, preferred_element_type=jnp.float32
    ) * head_size ** (-0.5)
    peak_score = jnp.maximum(largest, jnp.max(scores, axis=-1))
    shrink = jnp.exp(largest - peak_score)
    weights = jnp.exp(scores - peak_score[..., None])
    weight_sum = weight_sum * shrink + jnp.sum(weights, axis=-1)
    accumulated = accumulated * shrink[..., None] + jnp.einsum(
        "qgrk,kgd->qgrd",
        weights.astype(jnp.bfloat16),
        value_heads,
        preferred_element_type=jnp.float32,
    )
    return (peak_score, weight_sum, accumulated)


def attend_rows(state, queries, key_rows, value_rows):
    row_count = key_rows.shape[0]
    step_rows = block_rows(row_count, queries.shape[0])
    if step_rows == row_count:
        return attend_block(state, queries, key_rows, value_rows)

    def one_block(block_index, carried):
        offset = block_index * step_rows
        return attend_block(
            carried,
            queries,
            lax.dynamic_slice_in_dim(key_rows, offset, step_rows, 0),
            lax.dynamic_slice_in_dim(value_rows, offset, step_rows, 0),
        )

    return lax.fori_loop(0, row_count // step_rows, one_block, state)


def empty_state(queries):
    state_shape = queries.shape[:3]
    return (
        jnp.full(state_shape, -1e30, jnp.float32),
        jnp.zeros(state_shape, jnp.float32),
        jnp.zeros(queries.shape, jnp.float32),
    )


def finish(state):
    largest, weight_sum, accumulated = state
    merged = accumulated / weight_sum[..., None]
    return merged.reshape(merged.shape[0], -1).astype(jnp.bfloat16)


def on_device(
    queries_small,
    keys_small,
    values_small,
    queries_large,
    keys_large,
    values_large,
    query_gain_small,
    key_gain_small,
    query_gain_large,
    key_gain_large,
    residual_in,
    out_weight_small,
    out_weight_large,
    norm_gain,
    routes,
    route_scores,
    expert_gate,
    expert_up,
    expert_down,
):
    token_rows = queries_small.shape[0]
    offset = lax.axis_index("sp") * token_rows
    tables_small = grid_tables(offset, token_rows, HS_SMALL)
    tables_large = grid_tables(offset, token_rows, HS_LARGE)
    kv_small = keys_small.shape[1] // HS_SMALL
    kv_large = keys_large.shape[1] // HS_LARGE
    asked_small = normed_turn(
        queries_small.reshape(token_rows, -1, HS_SMALL), query_gain_small, tables_small
    ).reshape(token_rows, kv_small, -1, HS_SMALL)
    asked_large = normed_turn(
        queries_large.reshape(token_rows, -1, HS_LARGE), query_gain_large, tables_large
    ).reshape(token_rows, kv_large, -1, HS_LARGE)
    turned_small = normed_turn(
        keys_small.reshape(token_rows, kv_small, HS_SMALL), key_gain_small, tables_small
    ).reshape(token_rows, -1)
    turned_large = normed_turn(
        keys_large.reshape(token_rows, kv_large, HS_LARGE), key_gain_large, tables_large
    ).reshape(token_rows, -1)
    key_small = lax.all_gather(turned_small, "sp", axis=0, tiled=True)
    value_small = lax.all_gather(values_small, "sp", axis=0, tiled=True)
    key_large = lax.all_gather(turned_large, "sp", axis=0, tiled=True)
    value_large = lax.all_gather(values_large, "sp", axis=0, tiled=True)
    state_small = attend_rows(empty_state(asked_small), asked_small, key_small, value_small)
    state_large = attend_rows(empty_state(asked_large), asked_large, key_large, value_large)
    heard_small = finish(state_small)
    heard_large = finish(state_large)
    projected = lax.psum_scatter(
        (
            jnp.dot(heard_small, out_weight_small, preferred_element_type=jnp.float32)
            + jnp.dot(heard_large, out_weight_large, preferred_element_type=jnp.float32)
        ).astype(jnp.bfloat16),
        "tp",
        scatter_dimension=0,
        tiled=True,
    ).astype(jnp.float32)
    attended = (residual_in.astype(jnp.float32) + projected).astype(jnp.bfloat16)
    widened = attended.astype(jnp.float32)
    normed = (
        widened
        * lax.rsqrt(jnp.mean(widened * widened, axis=-1, keepdims=True) + norm_eps)
        * norm_gain
    ).astype(jnp.bfloat16)
    local_rows = routes.shape[0]
    top_count = routes.shape[1]
    sp_count = lax.axis_size("sp")
    local_experts = expert_gate.shape[0]
    expert_count = local_experts * sp_count
    capacity = max(2, (2 * top_count * local_rows + expert_count - 1) // expert_count)
    flat_routes = routes.reshape(-1)
    member = (flat_routes[:, None] == jnp.arange(expert_count, dtype=jnp.int32)[None, :]).astype(
        jnp.int32
    )
    ranks = jnp.sum((jnp.cumsum(member, axis=0) - member) * member, axis=1)
    slots = flat_routes * capacity + ranks
    picker = (
        slots[:, None] == jnp.arange(expert_count * capacity, dtype=jnp.int32)[None, :]
    ).astype(jnp.bfloat16)
    placer = jnp.sum(picker.reshape(local_rows, top_count, -1), axis=1)
    outgoing = jnp.einsum("ts,td->sd", placer, normed, preferred_element_type=jnp.float32).astype(
        jnp.bfloat16
    )
    outgoing = outgoing.reshape(sp_count, local_experts, capacity, -1)
    everyone = lax.all_gather(
        lax.all_to_all(outgoing, "sp", split_axis=0, concat_axis=0, tiled=True),
        "tp",
        axis=0,
        tiled=True,
    )
    gate_out = jnp.einsum(
        "secd,edf->secf", everyone, expert_gate, preferred_element_type=jnp.float32
    )
    up_out = jnp.einsum("secd,edf->secf", everyone, expert_up, preferred_element_type=jnp.float32)
    active = (jax.nn.silu(gate_out) * up_out).astype(jnp.bfloat16)
    summed = lax.psum_scatter(
        jnp.einsum(
            "secf,efd->secd", active, expert_down, preferred_element_type=jnp.float32
        ).astype(jnp.bfloat16),
        "tp",
        scatter_dimension=0,
        tiled=True,
    )
    returned = lax.all_to_all(summed, "sp", split_axis=0, concat_axis=0, tiled=True)
    back_rows = returned.reshape(expert_count * capacity, -1)
    chosen_rows = jnp.dot(picker, back_rows, preferred_element_type=jnp.float32).reshape(
        local_rows, top_count, -1
    )
    shares = route_scores / jnp.sum(route_scores, axis=1, keepdims=True)
    mixed = jnp.sum(chosen_rows * shares[:, :, None], axis=1)
    return (attended.astype(jnp.float32) + mixed).astype(jnp.bfloat16)


def solution(mesh):
    in_specs = (
        P(("grp", "sp"), "tp"),
        P(("grp", "sp"), "tp"),
        P(("grp", "sp"), "tp"),
        P(("grp", "sp"), "tp"),
        P(("grp", "sp"), "tp"),
        P(("grp", "sp"), "tp"),
        P("grp"),
        P("grp"),
        P("grp"),
        P("grp"),
        P(("grp", "sp", "tp"), None),
        P("tp", None),
        P("tp", None),
        P(),
        P(("grp", "sp", "tp"), None),
        P(("grp", "sp", "tp"), None),
        P("sp", None, "tp"),
        P("sp", None, "tp"),
        P("sp", "tp", None),
    )
    out_specs = P(("grp", "sp", "tp"), None)
    return jax.shard_map(
        on_device, mesh=mesh, in_specs=in_specs, out_specs=out_specs, check_vma=False
    )
```

profile of v0, /device:TPU:30, one launch (start us, length us, event | category | flops | bytes accessed | tf_op | source)
XLA Modules:
  0.0 308.8 jit_solution(7394251430156797041)
XLA Ops:
  6.6 1.1 copy.83
  9.8 14.5 %all_gather.17 = bf16[1024,128]{0,1:T(8,128)(2,1)S(1)} all-gather(bf16[256,128]{0,1:T(8,128)(2,1)S(1)} %pad_maximum_fusion.1), channel_id=1, replica_groups=mesh['grp'=2,'sp'=4,'tp'=4] {'sp'}, dimensions={0}, use_global_device_ids=true | all-gather | bytes 327680 | tf_op jit(solution)/shard_map/all_gather | solution.py:162
  26.6 1.3 copy-done.2
  28.4 13.9 %all_gather.18 = bf16[1024,128]{0,1:T(8,128)(2,1)S(1)} all-gather(bf16[256,128]{0,1:T(8,128)(2,1)S(1)} %copy.87), channel_id=1, replica_groups=mesh['grp'=2,'sp'=4,'tp'=4] {'sp'}, dimensions={0}, use_global_device_ids=true | all-gather | bytes 327680 | tf_op jit(solution)/shard_map/all_gather | solution.py:163
  42.8 14.2 %all_gather.15 = bf16[1024,128]{0,1:T(8,128)(2,1)S(1)} all-gather(bf16[256,128]{0,1:T(8,128)(2,1)S(1)} %bitcast.168), channel_id=1, replica_groups=mesh['grp'=2,'sp'=4,'tp'=4] {'sp'}, dimensions={0}, use_global_device_ids=true | all-gather | bytes 327680 | tf_op jit(solution)/shard_map/all_gather | solution.py:160
  58.8 1.2 copy-done.1
  60.1 13.9 %all_gather.16 = bf16[1024,128]{1,0:T(8,128)(2,1)S(1)} all-gather(bf16[256,128]{1,0:T(8,128)(2,1)S(1)} %copy-done.8), channel_id=1, replica_groups=mesh['grp'=2,'sp'=4,'tp'=4] {'sp'}, dimensions={0}, use_global_device_ids=true | all-gather | bytes 327680 | tf_op jit(solution)/shard_map/all_gather | solution.py:161
  74.1 3.1 fusion.38
  77.7 1.1 copy-done.3
  79.4 1.5 fusion.3
  81.9 23.8 %reduce-scatter.5.cloned.1.call-done = bf16[64,2048]{1,0:T(8,128)(2,1)} async-done(((bf16[256,2048]{1,0:T(8,128)(2,1)}), bf16[64,2048]{1,0:T(8,128)(2,1)}) %reduce-scatter.5.cloned.1.call-update) | async-done | bytes 262160 | tf_op jit(solution)/shard_map/reduce_scatter | solution.py:168
  105.8 1.1 fusion.48
  106.9 1.4 convolution_convert_fusion
  108.4 28.1 %all_to_all.10 = bf16[4,2,32,2048]{3,2,1,0:T(8,128)(2,1)S(1)} all-to-all(bf16[4,2,32,2048]{3,2,1,0:T(8,128)(2,1)S(1)} %bitcast.163), channel_id=1, replica_groups=mesh['grp'=2,'sp'=4,'tp'=4] {'sp'}, dimensions={0} | all-to-all | bytes 2097152 | tf_op jit(solution)/shard_map/all_to_all | solution.py:205
  136.5 1.0 copy.91
  137.8 34.4 %all-gather.2.cloned.1.call-done = bf16[16,2,32,2048]{3,2,0,1:T(8,128)(2,1)} async-done(((bf16[4,2,32,2048]{3,2,0,1:T(8,128)(2,1)}), bf16[16,2,32,2048]{3,2,0,1:T(8,128)(2,1)}) %all-gather.2.cloned.1.call-update) | async-done | bytes 4194320 | tf_op jit(solution)/shard_map/all_gather | solution.py:204
  172.2 4.1 %fusion.14 = f32[16,2,32,256]{3,2,0,1:T(8,128)S(1)} fusion(bf16[16,2,32,2048]{3,2,0,1:T(8,128)(2,1)} %all-gather.2.cloned.1.call-done, bf16[2,2048,256]{2,1,0:T(8,128)(2,1)} %param.35), kind=kOutput, calls=%fused_computation.21 | convolution fusion | flops 1073741824 | bytes 7340032 | tf_op jit(solution)/shard_map/secd,edf->secf/dot_general | solution.py:210
  176.3 7.3 %convert_bitcast_fusion = bf16[16,2,32,2048]{3,2,0,1:T(8,128)(2,1)} fusion(bf16[2,256,2048]{2,1,0:T(8,128)(2,1)S(1)} %copy-done, bf16[16,2,32,2048]{3,2,0,1:T(8,128)(2,1)} %all-gather.2.cloned.1.call-done, bf16[2,2048,256]{2,1,0:T(8,128)(2,1)} %param.36, f32[16,2,32,256]{3,2,0,1:T(8,128)S(1)} %fusion.14), kind=kOutput, calls=%fused_computation.3 | convolution fusion | flops 2151153664 | bytes 13631488 | tf_op jit(solution)/shard_map/secf,efd->secd/dot_general | solution.py:216
  185.5 83.9 %all-reduce.3.cloned.1.call-done = bf16[16,2,32,2048]{3,2,0,1:T(8,128)(2,1)} async-done(((bf16[16,2,32,2048]{3,2,0,1:T(8,128)(2,1)}), bf16[16,2,32,2048]{3,2,0,1:T(8,128)(2,1)}) %all-reduce.3.cloned.1.call-update) | async-done | bytes 4194320
  269.4 1.3 constant_dynamic-slice_fusion
  270.7 1.1 copy.92
  271.8 5.1 %all-to-all-start.1 = ((bf16[4,2,32,2048]{3,2,1,0:T(8,128)(2,1)}), bf16[4,2,32,2048]{3,2,1,0:T(8,128)(2,1)S(1)}, u32[]{:S(2)}, u32[]{:S(2)}) async-start(bf16[4,2,32,2048]{3,2,1,0:T(8,128)(2,1)} %copy.92), calls=%async_computation.2 | async-start | bytes 2097152 | tf_op jit(solution)/shard_map/all_to_all | solution.py:223
  276.9 23.3 %all-to-all-done.1 = bf16[4,2,32,2048]{3,2,1,0:T(8,128)(2,1)S(1)} async-done(((bf16[4,2,32,2048]{3,2,1,0:T(8,128)(2,1)}), bf16[4,2,32,2048]{3,2,1,0:T(8,128)(2,1)S(1)}, u32[]{:S(2)}, u32[]{:S(2)}) %all-to-all-start.1) | async-done | bytes 1048608 | tf_op jit(solution)/shard_map/all_to_all | solution.py:223
  300.6 1.7 fusion.51
  (92 shorter events, 11.1 us)
Async XLA Ops:
  6.5 169.7 %copy-start = (bf16[2,256,2048]{2,1,0:T(8,128)(2,1)S(1)}, bf16[2,256,2048]{2,1,0:T(8,128)(2,1)}, u32[]{:S(2)}) copy-start(bf16[2,256,2048]{2,1,0:T(8,128)(2,1)} %param.37) | copy-start | bytes 6291460
  6.5 18.9 %copy-start.14 = (f32[128]{0:T(128)S(1)}, f32[128]{0:T(128)}, u32[]{:S(2)}) copy-start(f32[128]{0:T(128)} %param.27) | copy-start | bytes 1540
  6.5 99.2 %reduce-scatter.5.cloned.1.call-start = ((), (), s32[]{:S(2)}) async-start(), calls=%async_computation.3 | async-start | bytes 1310720 | tf_op jit(solution)/shard_map/reduce_scatter | solution.py:168
  25.9 2.4 copy-start.9
  25.9 16.6 %copy-start.10 = (bf16[256,128]{1,0:T(8,128)(2,1)S(1)}, bf16[256,128]{1,0:T(8,128)(2,1)}, u32[]{:S(2)}) copy-start(bf16[256,128]{1,0:T(8,128)(2,1)} %param.20) | copy-start | bytes 196612
  26.5 1.3 copy-start.2
  26.5 16.1 %copy-start.15 = (f32[64]{0:T(128)S(1)}, f32[64]{0:T(128)}, u32[]{:S(2)}) copy-start(f32[64]{0:T(128)} %param.26) | copy-start | bytes 772
  26.5 30.5 %copy-start.7 = (bf16[256,256]{1,0:T(8,128)(2,1)S(1)}, bf16[256,256]{1,0:T(8,128)(2,1)}, u32[]{:S(2)}) copy-start(bf16[256,256]{1,0:T(8,128)(2,1)} %param.19) | copy-start | bytes 393220
  26.6 30.6 %copy-start.16 = (f32[64]{0:T(128)S(1)}, f32[64]{0:T(128)}, u32[]{:S(2)}) copy-start(f32[64]{0:T(128)} %param.25) | copy-start | bytes 772
  58.1 1.9 copy-start.1
  58.1 1.9 copy-start.8
  74.1 3.1 %copy-start.5 = (bf16[256,2048]{1,0:T(8,128)(2,1)S(1)}, bf16[256,2048]{1,0:T(8,128)(2,1)}, u32[]{:S(2)}) copy-start(bf16[256,2048]{1,0:T(8,128)(2,1)} %param.30) | copy-start | bytes 3145732
  77.2 1.6 copy-start.3
  77.7 1.6 copy-start.6
  79.3 1.6 copy-start.12
  79.3 26.4 %copy-start.4 = (bf16[64,2048]{1,0:T(8,128)(2,1)S(1)}, bf16[64,2048]{1,0:T(8,128)(2,1)}, u32[]{:S(2)}) copy-start(bf16[64,2048]{1,0:T(8,128)(2,1)} %param.29) | copy-start | bytes 786436
  79.4 27.6 %copy-start.11 = (f32[2048]{0:T(1024)S(1)}, f32[2048]{0:T(1024)}, u32[]{:S(2)}) copy-start(f32[2048]{0:T(1024)} %param.32) | copy-start | bytes 24580
  80.9 91.3 %all-gather.2.cloned.1.call-start = ((), (), s32[]{:S(2)}) async-start(), calls=%async_computation.4 | async-start | bytes 5242880 | tf_op jit(solution)/shard_map/all_gather | solution.py:204
  137.5 131.9 %all-reduce.3.cloned.1.call-start = ((), (), s32[]{:S(2)}) async-start(), calls=%async_computation.5 | async-start | bytes 8388608
  183.6 0.7 copy-start.17
  270.7 6.2 %copy-start.13 = (f32[64,2]{0,1:T(2,128)S(1)}, f32[64,2]{0,1:T(2,128)}, u32[]{:S(2)}) copy-start(f32[64,2]{0,1:T(2,128)} %param.34) | copy-start | bytes 1540
  271.8 28.4 %all-to-all-start.1 = ((bf16[4,2,32,2048]{3,2,1,0:T(8,128)(2,1)}), bf16[4,2,32,2048]{3,2,1,0:T(8,128)(2,1)S(1)}, u32[]{:S(2)}, u32[]{:S(2)}) async-start(bf16[4,2,32,2048]{3,2,1,0:T(8,128)(2,1)} %copy.92), calls=%async_computation.2 | async-start | bytes 2097152 | tf_op jit(solution)/shard_map/all_to_all | solution.py:223
Sparse Core Ops, SparseCore 0:
  81.0 24.7 reduce-scatter.4
  137.7 34.4 all-gather.1
  183.7 85.6 all-reduce.2
where the time goes:
time: 313 us; the launch traced here: 309 us
  waiting for transfers between devices  166 us (53%)
  blocking collectives  84.6 us (27%)
  matrix products  20.1 us (6%)
  between operations  14.3 us (5%)
  local copies, waits for them, and re-layouts  11.3 us (4%)
  other arithmetic  7.66 us (2%)
  starting transfers between devices  5.36 us (2%)
    unnamed x4, waiting for transfers between devices  84 us
    all_gather x1, waiting for transfers between devices, on_device(): lax.all_gather(lax.all_to_all(outgoing, 'sp', split_axis=0, concat_axis=0...  34.4 us
    all_to_all x1, blocking collectives, on_device(): lax.all_to_all(outgoing, 'sp', split_axis=0, concat_axis=0, tiled=True)  28.1 us
    reduce_scatter x1, waiting for transfers between devices, on_device(): lax.psum_scatter((jnp.dot(heard_small, out_weight_small, preferred_elemen...  23.8 us
    all_to_all x1, waiting for transfers between devices, on_device(): lax.all_to_all(summed, 'sp', split_axis=0, concat_axis=0, tiled=True)  23.3 us
    all_gather x1, blocking collectives, on_device(): key_large = lax.all_gather(turned_large, 'sp', axis=0, tiled=True)  14.5 us
    all_gather x1, blocking collectives, on_device(): key_small = lax.all_gather(turned_small, 'sp', axis=0, tiled=True)  14.2 us
    all_gather x1, blocking collectives, on_device(): value_large = lax.all_gather(values_large, 'sp', axis=0, tiled=True)  13.9 us
  transfers between devices with their start and end apart: 4, of which 4 were waited for; matrix products, arithmetic and copies ran while one was open for 1% of the time, Pallas kernels for 0%

commit v1 on v0

--- a/solution.py
+++ b/solution.py
@@ -1,6 +1,11 @@
+import functools
+
 import jax
 import jax.numpy as jnp
+import numpy as np
 from jax import lax
+from jax.experimental import pallas as pl
+from jax.experimental.pallas import tpu as pltpu
 from jax.sharding import PartitionSpec as P
 
 HS_SMALL = 64
@@ -230,6 +235,466 @@
     return (attended.astype(jnp.float32) + mixed).astype(jnp.bfloat16)
 
 
+MESH = pl.DeviceIdType.MESH
+LANES = 128
+
+
+def rotary_tables(grid_rows, head_size):
+    lane = np.arange(LANES) % head_size
+    rates = np.power(
+        np.float32(theta_base),
+        (np.float32(-2.0) * np.arange(head_size // 4, dtype=np.float32) / np.float32(head_size // 2)),
+    ).astype(np.float32)
+    rate = rates[lane % (head_size // 4)]
+    is_row = lane < head_size // 2
+    sign = np.where(lane % (head_size // 2) < head_size // 4, -1.0, 1.0)
+
+    def build(count, keep):
+        angles = np.arange(count, dtype=np.float32)[:, None] * rate[None, :]
+        angles = angles.astype(np.float64)
+        return (
+            np.where(keep, np.cos(angles), 0.0).astype(np.float32),
+            np.where(keep, np.sin(angles) * sign, 0.0).astype(np.float32),
+        )
+
+    return build(grid_rows, is_row), build(GRID_W, ~is_row)
+
+
+def visit_order(count):
+    return [sorted(range(count), key=lambda b: (abs(b - at), b)) for at in range(count)]
+
+
+def pick(table, at, step):
+    chosen = jnp.int32(0)
+    for i, row in enumerate(table):
+        for j, entry in enumerate(row):
+            chosen = jnp.where((at == i) & (step == j), jnp.int32(entry), chosen)
+    return chosen
+
+
+def lanes_of(shape):
+    return lax.broadcasted_iota(jnp.int32, shape, len(shape) - 1)
+
+
+def turn_rows(raw, gain, cosine, sine, head_size):
+    wide = raw.astype(jnp.float32)
+    lane = lanes_of(wide.shape)
+    squares = wide * wide
+    if head_size == LANES:
+        scale = lax.rsqrt(jnp.sum(squares, axis=-1, keepdims=True) / head_size + norm_eps)
+    else:
+        low = lane < head_size
+        first = jnp.sum(jnp.where(low, squares, 0.0), axis=-1, keepdims=True) / head_size
+        second = jnp.sum(jnp.where(low, 0.0, squares), axis=-1, keepdims=True) / head_size
+        scale = jnp.where(low, lax.rsqrt(first + norm_eps), lax.rsqrt(second + norm_eps))
+    scaled = wide * scale * gain
+    quarter = head_size // 4
+    ahead = pltpu.roll(scaled, LANES - quarter, 1)
+    behind = pltpu.roll(scaled, quarter, 1)
+    partner = jnp.where(lane % (2 * quarter) < quarter, ahead, behind)
+    return scaled * cosine + partner * sine
+
+
+def layer_kernel(
+    sp_count,
+    q_s, k_s, v_s, q_l, k_l, v_l, gains, row_tab, col_tab, residual, norm_gain, routes, scores,
+    ws_any, wl_any, eg_any, eu_any, ed_any,
+    out,
+    kv, qst, big, den, acc, heard, w_out, w_gate, w_up, w_down,
+    p_out, p_in, x_out, x_in, att, ag,
+    y_out, y_in, s1, xs, rx, zs, rz,
+    w_sem, kv_send, kv_recv, p_send, p_recv, ag_send, ag_fwd, ag_recv,
+    yc_send, yc_recv, rx_send, rx_recv, rz_send, rz_recv,
+):
+    n = sp_count
+    z = lax.axis_index("sp")
+    tp = lax.axis_index("tp")
+    x, c = tp // 2, tp % 2
+    sibling = {"tp": x * 2 + (1 - c)}
+    across = {"tp": (1 - x) * 2 + c}
+    order = visit_order(n)
+    tokens = q_s.shape[0]
+    rows = residual.shape[0]
+    width = residual.shape[1]
+    experts_here = eg_any.shape[0]
+    hidden = eg_any.shape[2]
+
+    def remote(src, dst, send, recv, to):
+        return pltpu.make_async_remote_copy(
+            src_ref=src, dst_ref=dst, send_sem=send, recv_sem=recv, device_id=to, device_id_type=MESH
+        )
+
+    half = ws_any.shape[0]
+    loads = [
+        pltpu.make_async_copy(ws_any, w_out.at[pl.ds(0, half)], w_sem.at[0]),
+        pltpu.make_async_copy(wl_any, w_out.at[pl.ds(half, half)], w_sem.at[1]),
+        pltpu.make_async_copy(eg_any, w_gate, w_sem.at[2]),
+        pltpu.make_async_copy(eu_any, w_up, w_sem.at[3]),
+        pltpu.make_async_copy(ed_any, w_down, w_sem.at[4]),
+    ]
+    for load in loads:
+        load.start()
+
+    barrier = pltpu.get_barrier_semaphore()
+    for away in range(1, n):
+        pl.semaphore_signal(barrier, inc=1, device_id={"sp": (z + away) % n}, device_id_type=MESH)
+    pl.semaphore_signal(barrier, inc=1, device_id=sibling, device_id_type=MESH)
+    pl.semaphore_signal(barrier, inc=1, device_id=across, device_id_type=MESH)
+
+    strips = tokens // GRID_W
+
+    def table(kind):
+        pieces = [
+            row_tab[kind, pl.ds(z * strips + r, 1), :] + col_tab[kind] for r in range(strips)
+        ]
+        return jnp.concatenate(pieces, axis=0)
+
+    cos_s, sin_s, cos_l, sin_l = table(0), table(1), table(2), table(3)
+    kv[z, 1] = v_s[...]
+    kv[z, 3] = v_l[...]
+    kv[z, 0] = turn_rows(k_s[...], gains[1:2, :], cos_s, sin_s, HS_SMALL).astype(jnp.bfloat16)
+    kv[z, 2] = turn_rows(k_l[...], gains[3:4, :], cos_l, sin_l, HS_LARGE).astype(jnp.bfloat16)
+    pl.semaphore_wait(barrier, n + 1)
+
+    def kv_copy(b, d):
+        return remote(
+            kv.at[b], kv.at[b], kv_send.at[b, (d + 1) // 2], kv_recv.at[b], {"sp": z + d}
+        )
+
+    for d in (1, -1):
+        @pl.when((z + d >= 0) & (z + d < n))
+        def _():
+            kv_copy(z, d).start()
+
+    low = lanes_of((tokens, LANES)) < HS_SMALL
+    zero = jnp.zeros((tokens, LANES), jnp.float32)
+    q01 = turn_rows(q_s[:, :LANES], gains[0:1, :], cos_s, sin_s, HS_SMALL)
+    q23 = turn_rows(q_s[:, LANES:], gains[0:1, :], cos_s, sin_s, HS_SMALL)
+    qst[0, :tokens] = jnp.where(low, q01, zero).astype(jnp.bfloat16)
+    qst[0, tokens:] = jnp.where(low, pltpu.roll(q01, HS_SMALL, 1), zero).astype(jnp.bfloat16)
+    qst[1, :tokens] = jnp.where(low, zero, pltpu.roll(q23, HS_SMALL, 1)).astype(jnp.bfloat16)
+    qst[1, tokens:] = jnp.where(low, zero, q23).astype(jnp.bfloat16)
+    for h in range(2):
+        piece = q_l[:, h * LANES : (h + 1) * LANES]
+        qst[2, h * tokens : (h + 1) * tokens] = turn_rows(
+            piece, gains[2:3, :], cos_l, sin_l, HS_LARGE
+        ).astype(jnp.bfloat16)
+    big[...] = jnp.full(big.shape, -1e30, jnp.float32)
+    den[...] = jnp.zeros(den.shape, jnp.float32)
+    acc[...] = jnp.zeros(acc.shape, jnp.float32)
+
+    def attend(j, carry):
+        b = pick(order, z, j)
+        d = jnp.where(b < z, 1, -1)
+
+        @pl.when(j > 0)
+        def _():
+            kv_copy(b, 1).wait_recv()
+
+            for way in (1, -1):
+                @pl.when((d == way) & (z + way >= 0) & (z + way < n))
+                def _():
+                    kv_copy(b, way).start()
+
+        for g in range(3):
+            keys = kv[b, 0 if g < 2 else 2]
+            values = kv[b, 1 if g < 2 else 3]
+            scale = (HS_SMALL if g < 2 else HS_LARGE) ** (-0.5)
+            score = (
+                lax.dot_general(
+                    qst[g], keys, (((1,), (1,)), ((), ())), preferred_element_type=jnp.float32
+                )
+                * scale
+            )
+            before = big[g]
+            peak = jnp.maximum(before, jnp.max(score, axis=-1, keepdims=True))
+            shrink = jnp.exp(before - peak)
+            weight = jnp.exp(score - peak[:, :1])
+            den[g] = den[g] * shrink + jnp.sum(weight, axis=-1, keepdims=True)
+            acc[g] = acc[g] * shrink + jnp.dot(
+                weight.astype(jnp.bfloat16), values, preferred_element_type=jnp.float32
+            )
+            big[g] = peak
+        return carry
+
+    lax.fori_loop(0, n, attend, 0)
+
+    o0, o1, o2 = acc[0] / den[0], acc[1] / den[1], acc[2] / den[2]
+    heard[:, 0:LANES] = jnp.where(low, o0[:tokens], pltpu.roll(o0[tokens:], HS_SMALL, 1)).astype(
+        jnp.bfloat16
+    )
+    heard[:, LANES : 2 * LANES] = jnp.where(
+        low, pltpu.roll(o1[:tokens], HS_SMALL, 1), o1[tokens:]
+    ).astype(jnp.bfloat16)
+    heard[:, 2 * LANES : 3 * LANES] = o2[:tokens].astype(jnp.bfloat16)
+    heard[:, 3 * LANES : 4 * LANES] = o2[tokens:].astype(jnp.bfloat16)
+
+    loads[0].wait()
+    loads[1].wait()
+
+    def projected(core):
+        lhs = jnp.concatenate(
+            [heard[pl.ds((xx * 2 + core) * rows, rows), :] for xx in range(2)], axis=0
+        )
+        return jnp.dot(lhs, w_out[...], preferred_element_type=jnp.float32).astype(jnp.bfloat16)
+
+    p_out[...] = projected(1 - c)
+    to_sibling = remote(p_out, p_in, p_send.at[0], p_recv.at[0], sibling)
+    to_sibling.start()
+    own_term = projected(c).astype(jnp.float32)
+    to_sibling.wait_recv()
+    pair = own_term + p_in[...].astype(jnp.float32)
+    here_first = x == 0
+    x_out[...] = jnp.where(here_first, pair[rows:], pair[:rows]).astype(jnp.bfloat16)
+    to_across = remote(x_out, x_in, p_send.at[1], p_recv.at[1], across)
+    to_across.start()
+    kept = jnp.where(here_first, pair[:rows], pair[rows:]) + residual[...].astype(jnp.float32)
+
+    share = scores[...] / jnp.sum(scores[...], axis=1, keepdims=True)
+    lane = lanes_of((rows, LANES))
+    dense = jnp.zeros((rows, LANES), jnp.float32)
+    for t in range(routes.shape[1]):
+        dense = jnp.where(lane == routes[:, t : t + 1], share[:, t : t + 1], dense)
+    dense_high = dense.astype(jnp.bfloat16).astype(jnp.float32)
+    packed = dense_high + pltpu.roll(dense - dense_high, LANES // 2, 1)
+    ag[z, x, c, :, width:] = packed.astype(jnp.bfloat16)
+
+    to_across.wait_recv()
+    attended = (kept + x_in[...].astype(jnp.float32)).astype(jnp.bfloat16)
+    att[...] = attended
+    wide = attended.astype(jnp.float32)
+    ag[z, x, c, :, :width] = (
+        wide
+        * lax.rsqrt(jnp.sum(wide * wide, axis=-1, keepdims=True) / width + norm_eps)
+        * norm_gain[...]
+    ).astype(jnp.bfloat16)
+
+    def ag_copy(b, xx, cc, sem, to):
+        block = ag.at[b, xx, cc]
+        return remote(block, block, sem, ag_recv.at[b, xx, cc], to)
+
+    def line_copy(b, d):
+        return ag_copy(b, x, c, ag_send.at[b, (d + 1) // 2], {"sp": z + d})
+
+    def spread(b):
+        return (
+            ag_copy(b, x, c, ag_send.at[b, 2], across),
+            ag_copy(b, x, c, ag_send.at[b, 3], sibling),
+        )
+
+    def forward(b):
+        return ag_copy(b, 1 - x, c, ag_fwd.at[b], sibling)
+
+    for d in (1, -1):
+        @pl.when((z + d >= 0) & (z + d < n))
+        def _():
+            line_copy(z, d).start()
+
+    for copy in spread(z):
+        copy.start()
+
+    def y_copy(b):
+        return remote(y_out.at[b], y_in.at[b], yc_send.at[b], yc_recv.at[b], sibling)
+
+    def x_copy(b):
+        return remote(xs.at[b], rx.at[b], rx_send.at[b], rx_recv.at[b], across)
+
+    def z_copy(b):
+        return remote(zs.at[b], rz.at[z], rz_send.at[b], rz_recv.at[z], {"sp": b})
+
+    def settle(b):
+        x_copy(b).wait_recv()
+        total = s1[b] + rx[b].astype(jnp.float32)
+
+        @pl.when(b == z)
+        def _():
+            s1[b] = total
+
+        @pl.when(b != z)
+        def _():
+            zs[b] = total.astype(jnp.bfloat16)
+            z_copy(b).start()
+
+    for load in loads[2:]:
+        load.wait()
+
+    def experts(j, carry):
+        b = pick(order, z, j)
+
+        @pl.when(j < n - 1)
+        def _():
+            later = pick(order, z, j + 1)
+            ag_copy(later, x, c, ag_send.at[later, 2], across).wait_recv()
+            for way in (1, -1):
+                @pl.when((jnp.where(later < z, 1, -1) == way) & (z + way >= 0) & (z + way < n))
+                def _():
+                    line_copy(later, way).start()
+
+            for copy in spread(later):
+                copy.start()
+
+        ag_copy(b, 1 - x, c, ag_fwd.at[b], sibling).wait_recv()
+        forward(b).start()
+        for xx in (x, 1 - x):
+            ag_copy(b, xx, 1 - c, ag_fwd.at[b], sibling).wait_recv()
+        blocks = [ag[b, xx, cc] for cc in (1 - c, c) for xx in range(2)]
+        rows_in = jnp.concatenate([block[:, :width] for block in blocks], axis=0)
+        marks = jnp.concatenate([block[:, width:] for block in blocks], axis=0).astype(jnp.float32)
+        mark_lane = lanes_of(marks.shape) % (LANES // 2)
+        active = []
+        for e in range(experts_here):
+            gate = jnp.dot(rows_in, w_gate[e], preferred_element_type=jnp.float32)
+            up = jnp.dot(rows_in, w_up[e], preferred_element_type=jnp.float32)
+            weight = jnp.sum(
+                jnp.where(mark_lane == z * experts_here + e, marks, 0.0), axis=1, keepdims=True
+            )
+            active.append((gate / (1.0 + jnp.exp(-gate)) * up * weight).astype(jnp.bfloat16))
+        hidden_rows = jnp.concatenate(active, axis=1)
+        down = w_down[...].reshape(experts_here * hidden, width)
+        split = 2 * rows
+        y_out[b] = jnp.dot(
+            hidden_rows[:split], down, preferred_element_type=jnp.float32
+        ).astype(jnp.bfloat16)
+        y_copy(b).start()
+        mine = jnp.dot(hidden_rows[split:], down, preferred_element_type=jnp.float32)
+        y_copy(b).wait_recv()
+        both = mine + y_in[b].astype(jnp.float32)
+        xs[b] = jnp.where(x == 0, both[rows:], both[:rows]).astype(jnp.bfloat16)
+        x_copy(b).start()
+        s1[b] = jnp.where(x == 0, both[:rows], both[rows:])
+
+        @pl.when(j > 0)
+        def _():
+            settle(pick(order, z, j - 1))
+
+        return carry
+
+    lax.fori_loop(0, n, experts, 0)
+    settle(pick(order, z, n - 1))
+
+    total = att[...].astype(jnp.float32) + s1[z]
+    for away in range(1, n):
+        source = (z + away) % n
+        remote(zs.at[source], rz.at[source], rz_send.at[source], rz_recv.at[source], {"sp": source}).wait_recv()
+        total = total + rz[source].astype(jnp.float32)
+    out[...] = total.astype(jnp.bfloat16)
+
+    to_sibling.wait_send()
+    to_across.wait_send()
+    for b in range(n):
+        for d in (1, -1):
+            @pl.when(((z - b) * d >= 0) & (z + d >= 0) & (z + d < n))
+            def _():
+                kv_copy(b, d).wait_send()
+                line_copy(b, d).wait_send()
+
+        for copy in spread(b):
+            copy.wait_send()
+        forward(b).wait_send()
+        y_copy(b).wait_send()
+        x_copy(b).wait_send()
+
+        @pl.when(b != z)
+        def _():
+            z_copy(b).wait_send()
+
+
+def layer_on_device(
+    queries_small, keys_small, values_small, queries_large, keys_large, values_large,
+    query_gain_small, key_gain_small, query_gain_large, key_gain_large,
+    residual_in, out_weight_small, out_weight_large, norm_gain, routes, route_scores,
+    expert_gate, expert_up, expert_down,
+):
+    n = lax.axis_size("sp")
+    tokens = queries_small.shape[0]
+    rows, width = residual_in.shape
+    experts_here, _, hidden = expert_gate.shape
+    grid_rows = n * tokens // GRID_W
+    small, large = rotary_tables(grid_rows, HS_SMALL), rotary_tables(grid_rows, HS_LARGE)
+    row_tab = jnp.asarray(np.stack([small[0][0], small[0][1], large[0][0], large[0][1]]))
+    col_tab = jnp.asarray(np.stack([small[1][0], small[1][1], large[1][0], large[1][1]]))
+    gains = jnp.stack(
+        [
+            jnp.tile(query_gain_small, LANES // HS_SMALL),
+            jnp.tile(key_gain_small, LANES // HS_SMALL),
+            query_gain_large,
+            key_gain_large,
+        ]
+    )
+    vmem = pl.BlockSpec(memory_space=pltpu.VMEM)
+    anywhere = pl.BlockSpec(memory_space=pl.ANY)
+    bf, f32 = jnp.bfloat16, jnp.float32
+    dma = pltpu.SemaphoreType.DMA
+    scratch = [
+        pltpu.VMEM((n, 4, tokens, LANES), bf),
+        pltpu.VMEM((3, 2 * tokens, LANES), bf),
+        pltpu.VMEM((3, 2 * tokens, LANES), f32),
+        pltpu.VMEM((3, 2 * tokens, LANES), f32),
+        pltpu.VMEM((3, 2 * tokens, LANES), f32),
+        pltpu.VMEM((tokens, 4 * LANES), bf),
+        pltpu.VMEM((2 * out_weight_small.shape[0], width), bf),
+        pltpu.VMEM(expert_gate.shape, bf),
+        pltpu.VMEM(expert_up.shape, bf),
+        pltpu.VMEM(expert_down.shape, bf),
+        pltpu.VMEM((2 * rows, width), bf),
+        pltpu.VMEM((2 * rows, width), bf),
+        pltpu.VMEM((rows, width), bf),
+        pltpu.VMEM((rows, width), bf),
+        pltpu.VMEM((rows, width), bf),
+        pltpu.VMEM((n, 2, 2, rows, width + LANES), bf),
+        pltpu.VMEM((n, 2 * rows, width), bf),
+        pltpu.VMEM((n, 2 * rows, width), bf),
+        pltpu.VMEM((n, rows, width), f32),
+        pltpu.VMEM((n, rows, width), bf),
+        pltpu.VMEM((n, rows, width), bf),
+        pltpu.VMEM((n, rows, width), bf),
+        pltpu.VMEM((n, rows, width), bf),
+        dma((5,)),
+        dma((n, 2)), dma((n,)),
+        dma((2,)), dma((2,)),
+        dma((n, 4)), dma((n,)), dma((n, 2, 2)),
+        dma((n,)), dma((n,)),
+        dma((n,)), dma((n,)),
+        dma((n,)), dma((n,)),
+    ]
+    return pl.pallas_call(
+        functools.partial(layer_kernel, n),
+        out_shape=jax.ShapeDtypeStruct((rows, width), bf),
+        in_specs=[vmem] * 13 + [anywhere] * 5,
+        out_specs=vmem,
+        scratch_shapes=scratch,
+        compiler_params=pltpu.CompilerParams(
+            collective_id=0, has_side_effects=True, vmem_limit_bytes=60 * 1024 * 1024
+        ),
+    )(
+        queries_small, keys_small, values_small, queries_large, keys_large, values_large,
+        gains, row_tab, col_tab, residual_in, norm_gain.reshape(1, width), routes, route_scores,
+        out_weight_small, out_weight_large, expert_gate, expert_up, expert_down,
+    )
+
+
+def choose(mesh, *arrays):
+    sp_count, tp_count = mesh.shape["sp"], mesh.shape["tp"]
+    rows, top_count = arrays[14].shape
+    experts_here = arrays[16].shape[0]
+    expert_count = experts_here * sp_count
+    capacity = max(2, (2 * top_count * rows + expert_count - 1) // expert_count)
+    tokens = arrays[0].shape[0]
+    fits = (
+        tp_count == 4
+        and expert_count <= LANES // 2
+        and tokens == tp_count * rows
+        and tokens % GRID_W == 0
+        and arrays[1].shape[1] == LANES
+        and arrays[4].shape[1] == LANES
+        and arrays[0].shape[1] == 2 * LANES
+        and arrays[3].shape[1] == 2 * LANES
+    )
+    if fits and experts_here * capacity >= rows:
+        return layer_on_device(*arrays)
+    return on_device(*arrays)
+
+
 def solution(mesh):
     in_specs = (
         P(("grp", "sp"), "tp"),
@@ -254,5 +719,5 @@
     )
     out_specs = P(("grp", "sp", "tp"), None)
     return jax.shard_map(
-        on_device, mesh=mesh, in_specs=in_specs, out_specs=out_specs, check_vma=False
-    )
+        functools.partial(choose, mesh), mesh=mesh, in_specs=in_specs, out_specs=out_specs, check_vma=False
+    )

time: 313 us -> 114 us (0.36); the launches traced: 309 us -> 114 us
  waiting for transfers between devices: 166 us -> 0 us
  Pallas kernels: 0 us -> 107 us
  blocking collectives: 84.6 us -> 0 us
  matrix products: 20.1 us -> 0 us
  between operations: 14.3 us -> 0.01 us
  other arithmetic: 7.66 us -> 1.27 us
  local copies, waits for them, and re-layouts: 11.3 us -> 5.89 us
  starting transfers between devices: 5.36 us -> 0 us
    pallas_call x0 -> x1, Pallas kernels: none -> 107 us  [layer_on_device(): pl.pallas_call(functools.partial(layer_kernel, n), out_shape=jax.ShapeDty...]
    unnamed x4 -> x0, waiting for transfers between devices: 84 us -> none
    all_gather x4 -> x0, blocking collectives: 56.5 us -> none  [the longest x1 14.5 us: on_device(): key_large = lax.all_gather(turned_large, 'sp', axis=0, tiled=True)]
    all_gather x1 -> x0, waiting for transfers between devices: 34.4 us -> none  [on_device(): lax.all_gather(lax.all_to_all(outgoing, 'sp', split_axis=0, concat_axis=0...]
    all_to_all x1 -> x0, blocking collectives: 28.1 us -> none  [on_device(): lax.all_to_all(outgoing, 'sp', split_axis=0, concat_axis=0, tiled=True)]
    reduce_scatter x1 -> x0, waiting for transfers between devices: 23.8 us -> none  [on_device(): lax.psum_scatter((jnp.dot(heard_small, out_weight_small, preferred_elemen...]
    all_to_all x1 -> x0, waiting for transfers between devices: 23.3 us -> none  [on_device(): lax.all_to_all(summed, 'sp', split_axis=0, concat_axis=0, tiled=True)]
    dot_general x10 -> x0, matrix products: 20.1 us -> none  [the longest x1 7.3 us: on_device(): jnp.einsum('secf,efd->secd', active, expert_down, preferred_element_type=...]
  transfers between devices with their start and end apart: 4 -> 0, of which waited for: 4 -> 0; matrix products, arithmetic and copies ran while one was open for 1% -> 0% of each run, Pallas kernels for 0% -> 0%
where the time goes in v1:
time: 114 us
  Pallas kernels  107 us (94%)
  local copies, waits for them, and re-layouts  5.89 us (5%)
  other arithmetic  1.27 us (1%)
    pallas_call x1, Pallas kernels, layer_on_device(): pl.pallas_call(functools.partial(layer_kernel, n), out_shape=jax.ShapeDty...  107 us
    unnamed x3, local copies, waits for them, and re-layouts  4.42 us

profile of v1, /device:TPU:30, one launch (start us, length us, event | category | flops | bytes accessed | tf_op | source)
XLA Modules:
  0.0 114.1 jit_solution(16668536186734322445)
XLA Ops:
  0.0 0.7 tile.4
  0.7 0.1 stack_tile.6
  0.7 0.7 tile.5
  1.4 0.1 stack_tile.7
  1.5 1.3 %pad_maximum_fusion.gains = f32[4,128]{1,0:T(4,128)} fusion(f32[1,128]{1,0:T(1,128)} %bitcast.4, f32[1,128]{1,0:T(1,128)} %bitcast.5, f32[1,128]{1,0:T(1,128)S(1)} %stack_tile.7, f32[1,128]{1,0:T(1,128)S(1)} %stack_tile.6), kind=kLoop, calls=%fused_computation | loop fusion | flops 1536 | bytes 4096 | tf_op jit(solution)/shard_map/stack | solution.py:616
  2.8 1.4 %copy.22.routes = s32[64,2]{1,0:T(8,128)} copy(s32[64,2]{0,1:T(2,128)} %param.35) | data formatting | bytes 1024 | tf_op args[14]
  4.1 1.4 %copy.23.scores = f32[64,2]{1,0:T(8,128)} copy(f32[64,2]{0,1:T(2,128)} %param.36) | data formatting | bytes 1024 | tf_op args[15]
  5.5 106.9 %shard_map.199 = bf16[64,2048]{1,0:T(8,128)(2,1)} custom-call(bf16[256,256]{1,0:T(8,128)(2,1)} %q_s.1, bf16[256,128]{1,0:T(8,128)(2,1)} %k_s.1, bf16[256,128]{1,0:T(8,128)(2,1)} %v_s.1, bf16[256,256]{1,0:T(8,128)(2,1)} %q_l.1, bf16[256,128]{1,0:T(8,128)(2,1)} %k_l.1, bf16[256,128]{1,0:T(8,128)(2,1)} %v_l.1, f32[4,128]{1,0:T(4,128)} %pad_maximum_fusion.gains, ...), custom_call_target="tpu_custom_call" | custom-call | tf_op jit(solution)/shard_map/pallas_call | solution.py:660
  112.4 1.7 %copy.25 = bf16[64,2048]{1,0:T(8,128)(2,1)} copy(bf16[64,2048]{1,0:T(8,128)(2,1)} %shard_map.199) | data formatting | bytes 524288

commit v2 on v1

--- a/solution.py
+++ b/solution.py
@@ -297,7 +297,7 @@
 
 def layer_kernel(
     sp_count,
-    q_s, k_s, v_s, q_l, k_l, v_l, gains, row_tab, col_tab, residual, norm_gain, routes, scores,
+    q_s, k_s, v_s, q_l, k_l, v_l, gain_qs, gain_ks, gain_ql, gain_kl, row_tab, col_tab, residual, norm_gain, routes, scores,
     ws_any, wl_any, eg_any, eu_any, ed_any,
     out,
     kv, qst, big, den, acc, heard, w_out, w_gate, w_up, w_down,
@@ -349,27 +349,39 @@
         ]
         return jnp.concatenate(pieces, axis=0)
 
+    kv[z, 0, 0] = v_s[...]
+    kv[z, 0, 1] = v_l[...]
     cos_s, sin_s, cos_l, sin_l = table(0), table(1), table(2), table(3)
-    kv[z, 1] = v_s[...]
-    kv[z, 3] = v_l[...]
-    kv[z, 0] = turn_rows(k_s[...], gains[1:2, :], cos_s, sin_s, HS_SMALL).astype(jnp.bfloat16)
-    kv[z, 2] = turn_rows(k_l[...], gains[3:4, :], cos_l, sin_l, HS_LARGE).astype(jnp.bfloat16)
+
+    def kv_copy(b, kind, d):
+        block = kv.at[b, kind]
+        return remote(
+            block, block, kv_send.at[b, kind, (d + 1) // 2], kv_recv.at[b, kind], {"sp": z + d}
+        )
+
+    def kv_start(b, kind, ways):
+        for d in (1, -1):
+            @pl.when(((ways == 0) | (ways == d)) & (z + d >= 0) & (z + d < n))
+            def _():
+                kv_copy(b, kind, d).start()
+
     pl.semaphore_wait(barrier, n + 1)
-
-    def kv_copy(b, d):
-        return remote(
-            kv.at[b], kv.at[b], kv_send.at[b, (d + 1) // 2], kv_recv.at[b], {"sp": z + d}
-        )
-
-    for d in (1, -1):
-        @pl.when((z + d >= 0) & (z + d < n))
-        def _():
-            kv_copy(z, d).start()
+    kv_start(z, 0, 0)
+
+    def both_heads(gain):
+        return jnp.concatenate([gain[...]] * (LANES // HS_SMALL), axis=1)
+
+    kv[z, 1, 0] = turn_rows(k_s[...], both_heads(gain_ks), cos_s, sin_s, HS_SMALL).astype(
+        jnp.bfloat16
+    )
+    kv[z, 1, 1] = turn_rows(k_l[...], gain_kl[...], cos_l, sin_l, HS_LARGE).astype(jnp.bfloat16)
+    kv_start(z, 1, 0)
+    inner = (z > 0) & (z < n - 1)
 
     low = lanes_of((tokens, LANES)) < HS_SMALL
     zero = jnp.zeros((tokens, LANES), jnp.float32)
-    q01 = turn_rows(q_s[:, :LANES], gains[0:1, :], cos_s, sin_s, HS_SMALL)
-    q23 = turn_rows(q_s[:, LANES:], gains[0:1, :], cos_s, sin_s, HS_SMALL)
+    q01 = turn_rows(q_s[:, :LANES], both_heads(gain_qs), cos_s, sin_s, HS_SMALL)
+    q23 = turn_rows(q_s[:, LANES:], both_heads(gain_qs), cos_s, sin_s, HS_SMALL)
     qst[0, :tokens] = jnp.where(low, q01, zero).astype(jnp.bfloat16)
     qst[0, tokens:] = jnp.where(low, pltpu.roll(q01, HS_SMALL, 1), zero).astype(jnp.bfloat16)
     qst[1, :tokens] = jnp.where(low, zero, pltpu.roll(q23, HS_SMALL, 1)).astype(jnp.bfloat16)
@@ -377,28 +389,33 @@
     for h in range(2):
         piece = q_l[:, h * LANES : (h + 1) * LANES]
         qst[2, h * tokens : (h + 1) * tokens] = turn_rows(
-            piece, gains[2:3, :], cos_l, sin_l, HS_LARGE
+            piece, gain_ql[...], cos_l, sin_l, HS_LARGE
         ).astype(jnp.bfloat16)
     big[...] = jnp.full(big.shape, -1e30, jnp.float32)
     den[...] = jnp.zeros(den.shape, jnp.float32)
     acc[...] = jnp.zeros(acc.shape, jnp.float32)
 
+    def take(j):
+        b = pick(order, z, j)
+        d = jnp.where(b < z, 1, -1)
+        for kind in range(2):
+            kv_copy(b, kind, 1).wait_recv()
+            kv_start(b, kind, d)
+
     def attend(j, carry):
         b = pick(order, z, j)
-        d = jnp.where(b < z, 1, -1)
-
-        @pl.when(j > 0)
-        def _():
-            kv_copy(b, 1).wait_recv()
-
-            for way in (1, -1):
-                @pl.when((d == way) & (z + way >= 0) & (z + way < n))
-                def _():
-                    kv_copy(b, way).start()
+
+        @pl.when((j > 0) & ((j != 2) | jnp.logical_not(inner)))
+        def _():
+            take(j)
+
+        @pl.when((j == 1) & inner)
+        def _():
+            take(2)
 
         for g in range(3):
-            keys = kv[b, 0 if g < 2 else 2]
-            values = kv[b, 1 if g < 2 else 3]
+            keys = kv[b, 1, 0 if g < 2 else 1]
+            values = kv[b, 0, 0 if g < 2 else 1]
             scale = (HS_SMALL if g < 2 else HS_LARGE) ** (-0.5)
             score = (
                 lax.dot_general(
@@ -432,36 +449,51 @@
     loads[0].wait()
     loads[1].wait()
 
-    def projected(core):
+    part = width // 2
+
+    def projected(core, h):
         lhs = jnp.concatenate(
             [heard[pl.ds((xx * 2 + core) * rows, rows), :] for xx in range(2)], axis=0
         )
-        return jnp.dot(lhs, w_out[...], preferred_element_type=jnp.float32).astype(jnp.bfloat16)
-
-    p_out[...] = projected(1 - c)
-    to_sibling = remote(p_out, p_in, p_send.at[0], p_recv.at[0], sibling)
-    to_sibling.start()
-    own_term = projected(c).astype(jnp.float32)
-    to_sibling.wait_recv()
-    pair = own_term + p_in[...].astype(jnp.float32)
+        return jnp.dot(
+            lhs, w_out[:, h * part : (h + 1) * part], preferred_element_type=jnp.float32
+        ).astype(jnp.bfloat16)
+
+    def p_copy(h):
+        return remote(p_out.at[h], p_in.at[h], p_send.at[0, h], p_recv.at[0, h], sibling)
+
+    def q_copy(h):
+        return remote(x_out.at[h], x_in.at[h], p_send.at[1, h], p_recv.at[1, h], across)
+
+    for h in range(2):
+        p_out[h] = projected(1 - c, h)
+        p_copy(h).start()
     here_first = x == 0
-    x_out[...] = jnp.where(here_first, pair[rows:], pair[:rows]).astype(jnp.bfloat16)
-    to_across = remote(x_out, x_in, p_send.at[1], p_recv.at[1], across)
-    to_across.start()
-    kept = jnp.where(here_first, pair[:rows], pair[rows:]) + residual[...].astype(jnp.float32)
-
-    share = scores[...] / jnp.sum(scores[...], axis=1, keepdims=True)
-    lane = lanes_of((rows, LANES))
-    dense = jnp.zeros((rows, LANES), jnp.float32)
-    for t in range(routes.shape[1]):
-        dense = jnp.where(lane == routes[:, t : t + 1], share[:, t : t + 1], dense)
+    for h in range(2):
+        own_term = projected(c, h).astype(jnp.float32)
+        p_copy(h).wait_recv()
+        pair = own_term + p_in[h].astype(jnp.float32)
+        x_out[h] = jnp.where(here_first, pair[rows:], pair[:rows]).astype(jnp.bfloat16)
+        q_copy(h).start()
+        cols = slice(h * part, (h + 1) * part)
+        s1[0, :, cols] = jnp.where(here_first, pair[:rows], pair[rows:]) + residual[
+            :, cols
+        ].astype(jnp.float32)
+
+    share = scores[...] / jnp.sum(scores[...], axis=0, keepdims=True)
+    names = lax.broadcasted_iota(jnp.int32, (LANES // 2, rows), 0)
+    dense = jnp.zeros((LANES // 2, rows), jnp.float32)
+    for t in range(routes.shape[0]):
+        dense = jnp.where(names == routes[t : t + 1, :], share[t : t + 1, :], dense)
     dense_high = dense.astype(jnp.bfloat16).astype(jnp.float32)
-    packed = dense_high + pltpu.roll(dense - dense_high, LANES // 2, 1)
-    ag[z, x, c, :, width:] = packed.astype(jnp.bfloat16)
-
-    to_across.wait_recv()
-    attended = (kept + x_in[...].astype(jnp.float32)).astype(jnp.bfloat16)
-    att[...] = attended
+    packed = jnp.concatenate([dense_high, dense - dense_high], axis=0)
+    ag[z, x, c, :, width:] = jnp.transpose(packed).astype(jnp.bfloat16)
+
+    for h in range(2):
+        cols = slice(h * part, (h + 1) * part)
+        q_copy(h).wait_recv()
+        att[:, cols] = (s1[0, :, cols] + x_in[h].astype(jnp.float32)).astype(jnp.bfloat16)
+    attended = att[...]
     wide = attended.astype(jnp.float32)
     ag[z, x, c, :, :width] = (
         wide
@@ -521,9 +553,8 @@
     def experts(j, carry):
         b = pick(order, z, j)
 
-        @pl.when(j < n - 1)
-        def _():
-            later = pick(order, z, j + 1)
+        def gain_block(step):
+            later = pick(order, z, step)
             ag_copy(later, x, c, ag_send.at[later, 2], across).wait_recv()
             for way in (1, -1):
                 @pl.when((jnp.where(later < z, 1, -1) == way) & (z + way >= 0) & (z + way < n))
@@ -532,6 +563,16 @@
 
             for copy in spread(later):
                 copy.start()
+
+        ahead = j + jnp.where(inner & (j > 0), 2, 1)
+
+        @pl.when(ahead < n)
+        def _():
+            gain_block(ahead)
+
+        @pl.when(inner & (j == 0))
+        def _():
+            gain_block(2)
 
         ag_copy(b, 1 - x, c, ag_fwd.at[b], sibling).wait_recv()
         forward(b).start()
@@ -563,13 +604,14 @@
         x_copy(b).start()
         s1[b] = jnp.where(x == 0, both[:rows], both[rows:])
 
-        @pl.when(j > 0)
-        def _():
-            settle(pick(order, z, j - 1))
+        @pl.when(j > 1)
+        def _():
+            settle(pick(order, z, j - 2))
 
         return carry
 
     lax.fori_loop(0, n, experts, 0)
+    settle(pick(order, z, n - 2))
     settle(pick(order, z, n - 1))
 
     total = att[...].astype(jnp.float32) + s1[z]
@@ -579,13 +621,15 @@
         total = total + rz[source].astype(jnp.float32)
     out[...] = total.astype(jnp.bfloat16)
 
-    to_sibling.wait_send()
-    to_across.wait_send()
+    for h in range(2):
+        p_copy(h).wait_send()
+        q_copy(h).wait_send()
     for b in range(n):
         for d in (1, -1):
             @pl.when(((z - b) * d >= 0) & (z + d >= 0) & (z + d < n))
             def _():
-                kv_copy(b, d).wait_send()
+                for kind in range(2):
+                    kv_copy(b, kind, d).wait_send()
                 line_copy(b, d).wait_send()
 
         for copy in spread(b):
@@ -613,20 +657,16 @@
     small, large = rotary_tables(grid_rows, HS_SMALL), rotary_tables(grid_rows, HS_LARGE)
     row_tab = jnp.asarray(np.stack([small[0][0], small[0][1], large[0][0], large[0][1]]))
     col_tab = jnp.asarray(np.stack([small[1][0], small[1][1], large[1][0], large[1][1]]))
-    gains = jnp.stack(
-        [
-            jnp.tile(query_gain_small, LANES // HS_SMALL),
-            jnp.tile(key_gain_small, LANES // HS_SMALL),
-            query_gain_large,
-            key_gain_large,
-        ]
-    )
+    gains = [
+        gain.reshape(1, -1)
+        for gain in (query_gain_small, key_gain_small, query_gain_large, key_gain_large)
+    ]
     vmem = pl.BlockSpec(memory_space=pltpu.VMEM)
     anywhere = pl.BlockSpec(memory_space=pl.ANY)
     bf, f32 = jnp.bfloat16, jnp.float32
     dma = pltpu.SemaphoreType.DMA
     scratch = [
-        pltpu.VMEM((n, 4, tokens, LANES), bf),
+        pltpu.VMEM((n, 2, 2, tokens, LANES), bf),
         pltpu.VMEM((3, 2 * tokens, LANES), bf),
         pltpu.VMEM((3, 2 * tokens, LANES), f32),
         pltpu.VMEM((3, 2 * tokens, LANES), f32),
@@ -636,10 +676,10 @@
         pltpu.VMEM(expert_gate.shape, bf),
         pltpu.VMEM(expert_up.shape, bf),
         pltpu.VMEM(expert_down.shape, bf),
-        pltpu.VMEM((2 * rows, width), bf),
-        pltpu.VMEM((2 * rows, width), bf),
-        pltpu.VMEM((rows, width), bf),
-        pltpu.VMEM((rows, width), bf),
+        pltpu.VMEM((2, 2 * rows, width // 2), bf),
+        pltpu.VMEM((2, 2 * rows, width // 2), bf),
+        pltpu.VMEM((2, rows, width // 2), bf),
+        pltpu.VMEM((2, rows, width // 2), bf),
         pltpu.VMEM((rows, width), bf),
         pltpu.VMEM((n, 2, 2, rows, width + LANES), bf),
         pltpu.VMEM((n, 2 * rows, width), bf),
@@ -650,8 +690,8 @@
         pltpu.VMEM((n, rows, width), bf),
         pltpu.VMEM((n, rows, width), bf),
         dma((5,)),
-        dma((n, 2)), dma((n,)),
-        dma((2,)), dma((2,)),
+        dma((n, 2, 2)), dma((n, 2)),
+        dma((2, 2)), dma((2, 2)),
         dma((n, 4)), dma((n,)), dma((n, 2, 2)),
         dma((n,)), dma((n,)),
         dma((n,)), dma((n,)),
@@ -660,7 +700,7 @@
     return pl.pallas_call(
         functools.partial(layer_kernel, n),
         out_shape=jax.ShapeDtypeStruct((rows, width), bf),
-        in_specs=[vmem] * 13 + [anywhere] * 5,
+        in_specs=[vmem] * 16 + [anywhere] * 5,
         out_specs=vmem,
         scratch_shapes=scratch,
         compiler_params=pltpu.CompilerParams(
@@ -668,7 +708,7 @@
         ),
     )(
         queries_small, keys_small, values_small, queries_large, keys_large, values_large,
-        gains, row_tab, col_tab, residual_in, norm_gain.reshape(1, width), routes, route_scores,
+        *gains, row_tab, col_tab, residual_in, norm_gain.reshape(1, width), routes.T, route_scores.T,
         out_weight_small, out_weight_large, expert_gate, expert_up, expert_down,
     )
 
@@ -682,6 +722,7 @@
     tokens = arrays[0].shape[0]
     fits = (
         tp_count == 4
+        and sp_count > 1
         and expert_count <= LANES // 2
         and tokens == tp_count * rows
         and tokens % GRID_W == 0

time: 114 us -> 106 us (0.930)
  local copies, waits for them, and re-layouts: 5.89 us -> 1.67 us
  Pallas kernels: 107 us -> 104 us
  other arithmetic: 1.27 us -> 0 us
    unnamed x3 -> x1, local copies, waits for them, and re-layouts: 4.42 us -> 1.67 us
    pallas_call x1, Pallas kernels: 107 us -> 104 us  [layer_on_device(): pl.pallas_call(functools.partial(layer_kernel, n), out_shape=jax.ShapeDty...]
    another operation x4 -> x0, local copies, waits for them, and re-layouts: 1.48 us -> none  [the longest x1 0.66 us: layer_on_device(): jnp.tile(query_gain_small, LANES // HS_SMALL)]
    another operation x1 -> x0, other arithmetic: 1.27 us -> none  [layer_on_device(): jnp.stack([jnp.tile(query_gain_small, LANES // HS_SMALL), jnp.tile(key_ga...]
where the time goes in v2:
time: 106 us
  Pallas kernels  104 us (98%)
  local copies, waits for them, and re-layouts  1.67 us (2%)
    pallas_call x1, Pallas kernels, layer_on_device(): pl.pallas_call(functools.partial(layer_kernel, n), out_shape=jax.ShapeDty...  104 us

profile of v2, /device:TPU:30, one launch (start us, length us, event | category | flops | bytes accessed | tf_op | source)
XLA Modules:
  0.0 106.0 jit_solution(13325265526989056964)
XLA Ops:
  0.0 104.3 %shard_map.199 = bf16[64,2048]{1,0:T(8,128)(2,1)} custom-call(bf16[256,256]{1,0:T(8,128)(2,1)} %q_s.1, bf16[256,128]{1,0:T(8,128)(2,1)} %k_s.1, bf16[256,128]{1,0:T(8,128)(2,1)} %v_s.1, bf16[256,256]{1,0:T(8,128)(2,1)} %q_l.1, bf16[256,128]{1,0:T(8,128)(2,1)} %k_l.1, bf16[256,128]{1,0:T(8,128)(2,1)} %v_l.1, f32[1,64]{1,0:T(1,128)} %bitcast.10, ...), custom_call_target="tpu_custom_call" | custom-call | tf_op jit(solution)/shard_map/pallas_call | solution.py:700
  104.3 1.7 %copy.23 = bf16[64,2048]{1,0:T(8,128)(2,1)} copy(bf16[64,2048]{1,0:T(8,128)(2,1)} %shard_map.199) | data formatting | bytes 524288

commit v3 on v2

--- a/solution.py
+++ b/solution.py
@@ -550,29 +550,25 @@
     for load in loads[2:]:
         load.wait()
 
+    def gain_block(step):
+        later = pick(order, z, step)
+        ag_copy(later, x, c, ag_send.at[later, 2], across).wait_recv()
+        for way in (1, -1):
+            @pl.when((jnp.where(later < z, 1, -1) == way) & (z + way >= 0) & (z + way < n))
+            def _():
+                line_copy(later, way).start()
+
+        for copy in spread(later):
+            copy.start()
+
+    gain_block(1)
+
+    @pl.when(inner)
+    def _():
+        gain_block(2)
+
     def experts(j, carry):
         b = pick(order, z, j)
-
-        def gain_block(step):
-            later = pick(order, z, step)
-            ag_copy(later, x, c, ag_send.at[later, 2], across).wait_recv()
-            for way in (1, -1):
-                @pl.when((jnp.where(later < z, 1, -1) == way) & (z + way >= 0) & (z + way < n))
-                def _():
-                    line_copy(later, way).start()
-
-            for copy in spread(later):
-                copy.start()
-
-        ahead = j + jnp.where(inner & (j > 0), 2, 1)
-
-        @pl.when(ahead < n)
-        def _():
-            gain_block(ahead)
-
-        @pl.when(inner & (j == 0))
-        def _():
-            gain_block(2)
 
         ag_copy(b, 1 - x, c, ag_fwd.at[b], sibling).wait_recv()
         forward(b).start()
@@ -604,14 +600,19 @@
         x_copy(b).start()
         s1[b] = jnp.where(x == 0, both[:rows], both[rows:])
 
-        @pl.when(j > 1)
+        ahead = j + jnp.where(inner, 3, 2)
+
+        @pl.when(ahead < n)
         def _():
-            settle(pick(order, z, j - 2))
+            gain_block(ahead)
+
+        @pl.when(j > 0)
+        def _():
+            settle(pick(order, z, j - 1))
 
         return carry
 
     lax.fori_loop(0, n, experts, 0)
-    settle(pick(order, z, n - 2))
     settle(pick(order, z, n - 1))
 
     total = att[...].astype(jnp.float32) + s1[z]

time: 106 us -> 106 us (level)
  no operation moved by 1% of the time
where the time goes in v3:
time: 106 us
  Pallas kernels  104 us (98%)
  local copies, waits for them, and re-layouts  1.67 us (2%)
    pallas_call x1, Pallas kernels, layer_on_device(): pl.pallas_call(functools.partial(layer_kernel, n), out_shape=jax.ShapeDty...  104 us

profile of v3, /device:TPU:30, one launch (start us, length us, event | category | flops | bytes accessed | tf_op | source)
XLA Modules:
  0.0 105.6 jit_solution(9182476709053477699)
XLA Ops:
  0.0 103.9 %shard_map.199 = bf16[64,2048]{1,0:T(8,128)(2,1)} custom-call(bf16[256,256]{1,0:T(8,128)(2,1)} %q_s.1, bf16[256,128]{1,0:T(8,128)(2,1)} %k_s.1, bf16[256,128]{1,0:T(8,128)(2,1)} %v_s.1, bf16[256,256]{1,0:T(8,128)(2,1)} %q_l.1, bf16[256,128]{1,0:T(8,128)(2,1)} %k_l.1, bf16[256,128]{1,0:T(8,128)(2,1)} %v_l.1, f32[1,64]{1,0:T(1,128)} %bitcast.10, ...), custom_call_target="tpu_custom_call" | custom-call | tf_op jit(solution)/shard_map/pallas_call | solution.py:701
  103.9 1.7 %copy.23 = bf16[64,2048]{1,0:T(8,128)(2,1)} copy(bf16[64,2048]{1,0:T(8,128)(2,1)} %shard_map.199) | data formatting | bytes 524288
